TPU v7x, 32 devices: a whole 2x2x4 slice. The times are simulated.
32 devices in a mesh: sp: 8 (over z, x), dp: 4 (over y, core).
Axes of the slice: x: 2, y: 2, z: 4, core: 2. Of those that a mesh axis runs over, the one named last changes fastest.
Arguments:
- queries: bfloat16 [4, 1024, 16, 128], P('dp', 'sp'), may hold values from -6 to 6
- key_rows: bfloat16 [4, 1024, 4, 128], P('dp', 'sp'), may hold values from -6 to 6
- values: bfloat16 [4, 1024, 4, 128], P('dp', 'sp'), may hold values from -6 to 6
- query_gain: float32 [128], replicated, may hold values from 0.4 to 5
- key_gain: float32 [128], replicated, may hold values from 0.4 to 5
- out_weight: bfloat16 [2048, 2048], P('sp', 'dp'), may hold values from -0.125 to 0.125
- residual: bfloat16 [4, 1024, 2048], P('dp', 'sp'), may hold values from -6 to 6
- norm_gain: float32 [2048], replicated, may hold values from 0.1 to 1.9
- expert_gate: bfloat16 [8, 2048, 1792], P('sp'), may hold values from -0.125 to 0.125
- expert_up: bfloat16 [8, 2048, 1792], P('sp'), may hold values from -0.125 to 0.125
- expert_down: bfloat16 [8, 1792, 2048], P('sp'), may hold values from -0.125 to 0.125
- routes: int32 [4, 1024, 2], P('dp', 'sp'), may hold values from 0 to 7, all different within a row; in each aligned block of 64 rows (0 to 63, 64 to 127, ..., all dimensions but the last counted through in order) at most 32 rows name the same one
- route_weight: float32 [4, 1024, 2], P('dp', 'sp'), may hold values from 0.25 to 1
Outputs:
- layer_out: bfloat16 [4, 1024, 2048], P('dp', 'sp')
Inputs may be any that keep to these rules, and one draw needn't show every extreme that they name: `routes`: in each aligned block of 64 rows of one device, no expert is named by more than 32 entries, a bound that some block reaches; the two experts of a row differ.
All inputs are finite; a program needn't handle non-finite values.
Results may differ from a plain program's by a relative error of at most 0.0095.
The roundings to bfloat16 on the way count: a program that leaves them out, or rounds other values in their place, can miss the bound.
Values may be sent and summed in bfloat16 or wider, within the bound.
No kernel may reach another device: no remote copies, remote signals or barrier semaphores. Data moves between devices by JAX's collectives and lax.ppermute only.
A program may use at most 128 MiB of HBM per device.

v0:
```python
import jax
import jax.numpy as jnp
from jax import lax
from jax.sharding import PartitionSpec as P

GRID_W = 64
EPS = 1e-06
THETA = 10000.0


def rotate_half(vector, position):
    half_size = vector.shape[-1] // 2
    inverse = THETA ** (-jnp.arange(half_size, dtype=jnp.float32) / half_size)
    angles = position[:, None] * inverse[None, :]
    cosine = jnp.cos(angles)[:, None, :]
    sine_part = jnp.sin(angles)[:, None, :]
    first_part = vector[..., :half_size]
    second_part = vector[..., half_size:]
    return jnp.concatenate(
        [
            first_part * cosine - second_part * sine_part,
            first_part * sine_part + second_part * cosine,
        ],
        axis=-1,
    )


def normalize_rotate(vector, gain, positions):
    as_float = vector.astype(jnp.float32)
    scaled = (
        as_float * lax.rsqrt(jnp.mean(as_float * as_float, axis=-1, keepdims=True) + EPS) * gain
    )
    grid_row = (positions // GRID_W).astype(jnp.float32)
    column = (positions % GRID_W).astype(jnp.float32)
    quarter = scaled.shape[-1] // 2
    turned = jnp.concatenate(
        [rotate_half(scaled[..., :quarter], grid_row), rotate_half(scaled[..., quarter:], column)],
        axis=-1,
    )
    return turned.astype(jnp.bfloat16)


def softmax_rows(scores):
    row_max = jnp.max(scores, axis=-1, keepdims=True)
    exponent = jnp.exp(scores - row_max)
    return (exponent / jnp.sum(exponent, axis=-1, keepdims=True)).astype(jnp.bfloat16)


def attend_block(query_rows, key_rows, value_rows):
    scores = jnp.einsum(
        "qd,kd->qk", query_rows, key_rows, preferred_element_type=jnp.float32
    ) * query_rows.shape[-1] ** (-0.5)
    weights = softmax_rows(scores)
    return jnp.dot(weights, value_rows, preferred_element_type=jnp.float32).astype(jnp.bfloat16)


def attend_heads(head_query, head_key, head_value):
    length, head_count, head_width = head_query.shape
    block_size = min(512, length)
    outputs = []
    for head_index in range(head_count):
        key_slice = head_key[:, head_index]
        value_slice = head_value[:, head_index]
        query_blocks = head_query[:, head_index].reshape(
            length // block_size, block_size, head_width
        )

        def one_block(query_block):
            return attend_block(query_block, key_slice, value_slice)

        outputs.append(lax.map(one_block, query_blocks).reshape(length, head_width))
    return jnp.stack(outputs, axis=1)


def project_tokens(attended, out_weight):
    all_rows = lax.all_gather(attended[None], "dp", axis=0, tiled=True)
    local_cols = lax.all_gather(out_weight, "sp", axis=0, tiled=True)
    partial_cols = jnp.einsum(
        "std,dc->stc", all_rows, local_cols, preferred_element_type=jnp.float32
    )
    back_cols = lax.all_to_all(
        partial_cols.astype(jnp.bfloat16), "dp", split_axis=0, concat_axis=2, tiled=True
    ).astype(partial_cols.dtype)
    return back_cols[0]


def on_device(
    queries,
    key_rows,
    values,
    query_gain,
    key_gain,
    out_weight,
    residual,
    norm_gain,
    expert_gate,
    expert_up,
    expert_down,
    routes,
    route_weight,
):
    tok_count = queries.shape[1]
    head_count = queries.shape[2]
    head_width = queries.shape[3]
    group_size = head_count // key_rows.shape[2]
    positions = lax.axis_index("sp") * tok_count + jnp.arange(tok_count, dtype=jnp.int32)
    rot_query = normalize_rotate(queries[0], query_gain, positions)
    rot_key = normalize_rotate(key_rows[0], key_gain, positions)
    value_rows = values[0]
    head_query, head_key, head_value = (
        lax.all_to_all(rot_query, "sp", split_axis=1, concat_axis=0, tiled=True),
        lax.all_to_all(
            jnp.repeat(rot_key, group_size, axis=1), "sp", split_axis=1, concat_axis=0, tiled=True
        ),
        lax.all_to_all(
            jnp.repeat(value_rows, group_size, axis=1),
            "sp",
            split_axis=1,
            concat_axis=0,
            tiled=True,
        ),
    )
    by_heads = attend_heads(head_query, head_key, head_value)
    returned_heads = lax.all_to_all(by_heads, "sp", split_axis=0, concat_axis=1, tiled=True)
    projected = project_tokens(
        returned_heads.reshape(tok_count, head_count * head_width), out_weight
    )
    mixed_sum = residual[0].astype(jnp.float32) + projected
    normed = (
        mixed_sum
        * lax.rsqrt(jnp.mean(mixed_sum * mixed_sum, axis=-1, keepdims=True) + EPS)
        * norm_gain
    ).astype(jnp.bfloat16)
    experts = expert_gate.shape[0] * lax.axis_size("sp")
    half_rows = tok_count // 2
    capacity = max(2, 4 * half_rows // experts)
    chosen = routes[0].reshape(2, half_rows * 2)
    onehot = (chosen[..., None] == jnp.arange(experts, dtype=jnp.int32)).astype(jnp.int32)
    slot_rank = jnp.sum(jnp.cumsum(onehot, axis=1) * onehot, axis=-1) - 1
    slot_index = jnp.arange(2, dtype=jnp.int32)[:, None] * capacity + slot_rank
    target = (chosen * (2 * capacity) + slot_index).reshape(-1)
    model_width = normed.shape[1]
    filled = (
        jnp.zeros((experts * 2 * capacity, model_width), jnp.bfloat16)
        .at[target]
        .set(jnp.repeat(normed, 2, axis=0))
    )
    buffer = filled.reshape(experts, 2 * capacity, model_width)
    slot_batch = lax.all_to_all(buffer, "sp", split_axis=0, concat_axis=0, tiled=True)
    sources, slot_count, feature_count = slot_batch.shape
    flat_rows = slot_batch.reshape(sources * slot_count, feature_count)
    gate_part = jnp.dot(flat_rows, expert_gate[0], preferred_element_type=jnp.float32)
    up_part = jnp.dot(flat_rows, expert_up[0], preferred_element_type=jnp.float32)
    hidden = (jax.nn.silu(gate_part) * up_part).astype(jnp.bfloat16)
    expert_result = jnp.dot(hidden, expert_down[0], preferred_element_type=jnp.float32).astype(
        jnp.bfloat16
    )
    served = expert_result.reshape(sources, slot_count, feature_count)
    returned = lax.all_to_all(served, "sp", split_axis=0, concat_axis=0, tiled=True)
    picked = (
        returned.reshape(-1, model_width)[target]
        .astype(jnp.float32)
        .reshape(tok_count, 2, model_width)
    )
    result = mixed_sum + jnp.sum(picked * route_weight[0][..., None], axis=1)
    return result.astype(jnp.bfloat16)[None]


def solution(mesh):
    in_specs = (
        P("dp", "sp", None, None),
        P("dp", "sp", None, None),
        P("dp", "sp", None, None),
        P(),
        P(),
        P("sp", "dp"),
        P("dp", "sp", None),
        P(),
        P("sp", None, None),
        P("sp", None, None),
        P("sp", None, None),
        P("dp", "sp", None),
        P("dp", "sp", None),
    )
    out_specs = P("dp", "sp", None)
    return jax.shard_map(
        on_device, mesh=mesh, in_specs=in_specs, out_specs=out_specs, check_vma=False
    )
```

profile of v0, /device:TPU:0, one launch (start us, length us, event | category | flops | bytes accessed | tf_op | source)
XLA Modules:
  0.0 305.6 jit_solution(6616813318897419317)
XLA Ops:
  6.6 1.1 fusion.41
  7.7 1.1 fusion.42
  8.8 0.5 multiply_cosine_fusion.1
  9.4 0.5 subtract_convert_fusion.3
  9.9 0.4 pad_maximum_fusion.2
  10.3 0.9 broadcast_in_dim.14
  11.2 7.3 %all-to-all-start.1 = ((bf16[128,16,128]{2,0,1:T(8,128)(2,1)}), bf16[128,16,128]{2,0,1:T(8,128)(2,1)S(1)}, u32[]{:S(2)}, u32[]{:S(2)}) async-start(bf16[128,16,128]{2,0,1:T(8,128)(2,1)} %bitcast.12), calls=%async_computation.1 | async-start | bytes 1048576 | tf_op jit(solution)/shard_map/all_to_all | solution.py:112
  18.5 0.3 fusion.37
  18.9 0.3 fusion.38
  19.2 0.9 subtract_convert_fusion.1
  20.1 1.5 pad_maximum_fusion
  21.6 11.4 %all-to-all-done.1 = bf16[128,16,128]{2,0,1:T(8,128)(2,1)S(1)} async-done(((bf16[128,16,128]{2,0,1:T(8,128)(2,1)}), bf16[128,16,128]{2,0,1:T(8,128)(2,1)S(1)}, u32[]{:S(2)}, u32[]{:S(2)}) %all-to-all-start.1) | async-done | bytes 524320 | tf_op jit(solution)/shard_map/all_to_all | solution.py:112
  33.0 3.6 %all-to-all-start = ((bf16[128,16,128]{2,0,1:T(8,128)(2,1)}), bf16[128,16,128]{2,0,1:T(8,128)(2,1)S(1)}, u32[]{:S(2)}, u32[]{:S(2)}) async-start(bf16[128,16,128]{2,0,1:T(8,128)(2,1)} %pad_maximum_fusion), calls=%async_computation | async-start | bytes 1048576 | tf_op jit(solution)/shard_map/all_to_all | solution.py:111
  36.7 14.6 %all-to-all-done = bf16[128,16,128]{2,0,1:T(8,128)(2,1)S(1)} async-done(((bf16[128,16,128]{2,0,1:T(8,128)(2,1)}), bf16[128,16,128]{2,0,1:T(8,128)(2,1)S(1)}, u32[]{:S(2)}, u32[]{:S(2)}) %all-to-all-start) | async-done | bytes 524320 | tf_op jit(solution)/shard_map/all_to_all | solution.py:111
  51.3 0.9 broadcast_in_dim.15
  52.2 3.6 %all-to-all-start.2 = ((bf16[128,16,128]{2,0,1:T(8,128)(2,1)}), bf16[128,16,128]{2,0,1:T(8,128)(2,1)S(1)}, u32[]{:S(2)}, u32[]{:S(2)}) async-start(bf16[128,16,128]{2,0,1:T(8,128)(2,1)} %bitcast.18), calls=%async_computation.2 | async-start | bytes 1048576 | tf_op jit(solution)/shard_map/all_to_all | solution.py:115
  55.9 0.7 all-gather.5.cloned.1.call-update
  56.8 13.7 %all-to-all-done.2 = bf16[128,16,128]{2,0,1:T(8,128)(2,1)S(1)} async-done(((bf16[128,16,128]{2,0,1:T(8,128)(2,1)}), bf16[128,16,128]{2,0,1:T(8,128)(2,1)S(1)}, u32[]{:S(2)}, u32[]{:S(2)}) %all-to-all-start.2) | async-done | bytes 524320 | tf_op jit(solution)/shard_map/all_to_all | solution.py:115
  70.6 3.4 %while.20 = (s32[]{:T(128)}, bf16[2,512,128]{2,1,0:T(8,128)(2,1)S(1)}, bf16[2,512,128]{2,1,0:T(8,128)(2,1)S(1)}, bf16[1024,128]{1,0:T(8,128)(2,1)S(1)}, bf16[1024,128]{1,0:T(8,128)(2,1)S(1)}, /*index=5*/s32[]{:T(128)}) while((s32[]{:T(128)}, bf16[2,512,128]{2,1,0:T(8,128)(2,1)S(1)}, bf16[2,512,128]{2,1,0:T(8,128)(2,1)S(1)}, ...), condition=%wide.region_5.6_spmd, body=%wide.region_2.5_spmd.sunk | while | flops 273218560 | bytes 7088205 | solution.py:71
  70.6 0.5 multiply_reduce_fusion.6
  71.2 0.5 fusion.65
  71.7 0.7 fusion.66
  72.4 0.5 multiply_reduce_fusion.6
  72.9 0.5 fusion.65
  73.4 0.7 fusion.66
  74.1 3.5 %while.21 = (s32[]{:T(128)}, bf16[2,512,128]{2,1,0:T(8,128)(2,1)S(1)}, bf16[2,512,128]{2,1,0:T(8,128)(2,1)S(1)}, bf16[1024,128]{1,0:T(8,128)(2,1)S(1)}, bf16[1024,128]{1,0:T(8,128)(2,1)S(1)}, /*index=5*/s32[]{:T(128)}) while((s32[]{:T(128)}, bf16[2,512,128]{2,1,0:T(8,128)(2,1)S(1)}, bf16[2,512,128]{2,1,0:T(8,128)(2,1)S(1)}, ...), condition=%wide.region_9.10_spmd, body=%wide.region_6.9_spmd.sunk | while | flops 273218560 | bytes 7088205 | solution.py:71
  74.1 0.5 multiply_reduce_fusion.7
  74.7 0.5 fusion.69
  75.2 0.7 fusion.70
  75.9 0.5 multiply_reduce_fusion.7
  76.4 0.5 fusion.69
  76.9 0.7 fusion.70
  77.7 0.5 copy.114
  78.2 28.0 %all_to_all.88 = bf16[1024,2,128]{2,1,0:T(2,128)(2,1)S(1)} all-to-all(bf16[1024,2,128]{2,1,0:T(2,128)(2,1)S(1)} %copy.114), channel_id=1, replica_groups=mesh['sp'=8,'dp'=4] {'sp'}, dimensions={0} | all-to-all | bytes 1048576 | tf_op jit(solution)/shard_map/all_to_all | solution.py:124
  106.3 0.3 copy.116
  106.6 1.0 copy.117
  107.7 0.1 eq.18
  108.0 0.2 reduce_window_sum.11
  108.3 0.1 mul.319
  108.4 0.2 select_reduce_fusion
  108.6 5.1 %all-gather.5.cloned.1.call-done = bf16[2048,512]{1,0:T(8,128)(2,1)} async-done(((bf16[256,512]{1,0:T(8,128)(2,1)}), bf16[2048,512]{1,0:T(8,128)(2,1)}) %all-gather.5.cloned.1.call-update) | async-done | bytes 2097168 | tf_op jit(solution)/shard_map/all_gather | solution.py:77
  113.7 23.2 %all-gather.3.cloned.1.call-done = bf16[4,128,2048]{2,1,0:T(8,128)(2,1)} async-done(((bf16[1,128,2048]{2,1,0:T(8,128)(2,1)}), bf16[4,128,2048]{2,1,0:T(8,128)(2,1)}) %all-gather.3.cloned.1.call-update) | async-done | bytes 2097168 | tf_op jit(solution)/shard_map/all_gather | solution.py:76
  136.9 4.3 %fusion.29 = bf16[4,128,512]{2,1,0:T(8,128)(2,1)} fusion(bf16[4,128,2048]{2,1,0:T(8,128)(2,1)} %all-gather.3.cloned.1.call-done, bf16[2048,512]{1,0:T(8,128)(2,1)} %all-gather.5.cloned.1.call-done), kind=kOutput, calls=%fused_computation.41 | convolution fusion | flops 1074003968 | bytes 4718592 | tf_op jit(solution)/shard_map/std,dc->stc/dot_general | solution.py:78
  141.1 3.7 %all-to-all-start.4 = ((bf16[4,128,512]{2,1,0:T(8,128)(2,1)}), bf16[4,128,512]{2,1,0:T(8,128)(2,1)S(1)}, u32[]{:S(2)}, u32[]{:S(2)}) async-start(bf16[4,128,512]{2,1,0:T(8,128)(2,1)} %fusion.29), calls=%async_computation.4 | async-start | bytes 1048576 | tf_op jit(solution)/shard_map/all_to_all | solution.py:81
  144.9 8.5 %all-to-all-done.4 = bf16[4,128,512]{2,1,0:T(8,128)(2,1)S(1)} async-done(((bf16[4,128,512]{2,1,0:T(8,128)(2,1)}), bf16[4,128,512]{2,1,0:T(8,128)(2,1)S(1)}, u32[]{:S(2)}, u32[]{:S(2)}) %all-to-all-start.4) | async-done | bytes 524320 | tf_op jit(solution)/shard_map/all_to_all | solution.py:81
  153.4 0.1 convert_bitcast_fusion.1
  153.5 0.3 copy.118
  153.9 0.3 copy.123
  154.2 0.4 copy-done
  154.6 0.2 multiply_reduce_fusion.3
  154.8 0.2 multiply_convert_fusion.1
  155.0 0.6 broadcast_in_dim.17
  155.6 1.2 reshape.305
  156.9 3.5 %scatter_custom_fusion = bf16[512,2048]{1,0:T(8,128)(2,1)S(1)} fusion(s32[256]{0:T(256)S(1)} %bitcast.142, bf16[256,2048]{1,0:T(8,128)(2,1)} %reshape.305, bf16[]{:T(256)} %constant.89.clone.1), kind=kCustom, calls=%fused_computation.50 | custom fusion | bytes 2097664 | tf_op jit(solution)/shard_map/scatter | solution.py:146
  160.4 53.4 %all_to_all.89 = bf16[8,64,2048]{2,1,0:T(8,128)(2,1)} all-to-all(bf16[8,64,2048]{2,1,0:T(8,128)(2,1)S(1)} %bitcast.127), channel_id=1, replica_groups=mesh['sp'=8,'dp'=4] {'sp'}, dimensions={0} | all-to-all | bytes 4194304 | tf_op jit(solution)/shard_map/all_to_all | solution.py:149
  213.8 9.5 %fusion.20 = f32[512,1792]{1,0:T(8,128)} fusion(bf16[512,2048]{1,0:T(8,128)(2,1)} %bitcast.41, bf16[1,2048,1792]{2,1,0:T(8,128)(2,1)} %param.25), kind=kOutput, calls=%fused_computation.30 | convolution fusion | flops 3758096384 | bytes 13107200 | tf_op jit(solution)/shard_map/dot_general | solution.py:152
  223.3 17.0 %fusion.24 = bf16[512,2048]{1,0:T(8,128)(2,1)} fusion(bf16[1,1792,2048]{2,1,0:T(8,128)(2,1)} %param.27, f32[512,1792]{1,0:T(8,128)} %fusion.20, bf16[512,2048]{1,0:T(8,128)(2,1)} %bitcast.41, bf16[1,2048,1792]{2,1,0:T(8,128)(2,1)} %param.26), kind=kOutput, calls=%fused_computation.33 | convolution fusion | flops 7522746368 | bytes 22544384 | tf_op jit(solution)/shard_map/dot_general | solution.py:155
  240.3 4.0 %all-to-all-start.6 = ((bf16[8,64,2048]{2,1,0:T(8,128)(2,1)}), bf16[8,64,2048]{2,1,0:T(8,128)(2,1)S(1)}, u32[]{:S(2)}, u32[]{:S(2)}) async-start(bf16[8,64,2048]{2,1,0:T(8,128)(2,1)} %bitcast.130), calls=%async_computation.6 | async-start | bytes 4194304 | tf_op jit(solution)/shard_map/all_to_all | solution.py:159
  244.4 1.3 copy.119
  245.7 46.2 %all-to-all-done.6 = bf16[8,64,2048]{2,1,0:T(8,128)(2,1)S(1)} async-done(((bf16[8,64,2048]{2,1,0:T(8,128)(2,1)}), bf16[8,64,2048]{2,1,0:T(8,128)(2,1)S(1)}, u32[]{:S(2)}, u32[]{:S(2)}) %all-to-all-start.6) | async-done | bytes 2097184 | tf_op jit(solution)/shard_map/all_to_all | solution.py:159
  291.9 1.4 gather_fusion
  293.3 1.3 reshape.290
  294.6 3.2 %multiply_reduce_fusion.2 = f32[128,2048]{1,0:T(8,128)S(1)} fusion(f32[128,2,2048]{2,1,0:T(2,128)S(1)} %reshape.290, f32[128,2]{1,0:T(8,128)S(1)} %copy.124), kind=kLoop, calls=%fused_computation.36 | loop fusion | flops 786432 | bytes 3146752 | tf_op jit(solution)/shard_map/reduce_sum | solution.py:165
  297.8 1.0 fusion.35
  (46 shorter events, 1.2 us)
Async XLA Ops:
  9.4 9.1 %copy-start.3 = (bf16[1,128,16,128]{3,2,1,0:T(8,128)(2,1)S(1)}, bf16[1,128,16,128]{3,2,1,0:T(8,128)(2,1)}, u32[]{:S(2)}) copy-start(bf16[1,128,16,128]{3,2,1,0:T(8,128)(2,1)} %param.17) | copy-start | bytes 1572868
  9.4 9.5 %copy-start.8 = (f32[128]{0:T(128)S(1)}, f32[128]{0:T(128)}, u32[]{:S(2)}) copy-start(f32[128]{0:T(128)} %param.20) | copy-start | bytes 1540
  11.2 21.8 %all-to-all-start.1 = ((bf16[128,16,128]{2,0,1:T(8,128)(2,1)}), bf16[128,16,128]{2,0,1:T(8,128)(2,1)S(1)}, u32[]{:S(2)}, u32[]{:S(2)}) async-start(bf16[128,16,128]{2,0,1:T(8,128)(2,1)} %bitcast.12), calls=%async_computation.1 | async-start | bytes 1048576 | tf_op jit(solution)/shard_map/all_to_all | solution.py:112
  20.1 16.5 %copy-start.4 = (bf16[1,128,4,128]{3,2,1,0:T(4,128)(2,1)S(1)}, bf16[1,128,4,128]{3,2,1,0:T(4,128)(2,1)}, u32[]{:S(2)}) copy-start(bf16[1,128,4,128]{3,2,1,0:T(4,128)(2,1)} %param.19) | copy-start | bytes 393220
  33.0 18.3 %all-to-all-start = ((bf16[128,16,128]{2,0,1:T(8,128)(2,1)}), bf16[128,16,128]{2,0,1:T(8,128)(2,1)S(1)}, u32[]{:S(2)}, u32[]{:S(2)}) async-start(bf16[128,16,128]{2,0,1:T(8,128)(2,1)} %pad_maximum_fusion), calls=%async_computation | async-start | bytes 1048576 | tf_op jit(solution)/shard_map/all_to_all | solution.py:111
  52.2 18.3 %all-to-all-start.2 = ((bf16[128,16,128]{2,0,1:T(8,128)(2,1)}), bf16[128,16,128]{2,0,1:T(8,128)(2,1)S(1)}, u32[]{:S(2)}, u32[]{:S(2)}) async-start(bf16[128,16,128]{2,0,1:T(8,128)(2,1)} %bitcast.18), calls=%async_computation.2 | async-start | bytes 1048576 | tf_op jit(solution)/shard_map/all_to_all | solution.py:115
  55.8 57.9 %all-gather.5.cloned.1.call-start = ((), (), s32[]{:S(2)}) async-start(), calls=%async_computation.8 | async-start | bytes 2359296 | tf_op jit(solution)/shard_map/all_gather | solution.py:77
  56.6 80.3 %all-gather.3.cloned.1.call-start = ((), (), s32[]{:S(2)}) async-start(), calls=%async_computation.7 | async-start | bytes 2621440 | tf_op jit(solution)/shard_map/all_gather | solution.py:76
  106.2 1.4 copy-start.6
  141.1 12.3 %all-to-all-start.4 = ((bf16[4,128,512]{2,1,0:T(8,128)(2,1)}), bf16[4,128,512]{2,1,0:T(8,128)(2,1)S(1)}, u32[]{:S(2)}, u32[]{:S(2)}) async-start(bf16[4,128,512]{2,1,0:T(8,128)(2,1)} %fusion.29), calls=%async_computation.4 | async-start | bytes 1048576 | tf_op jit(solution)/shard_map/all_to_all | solution.py:81
  153.5 1.0 copy-start
  153.9 0.9 copy-start.5
  240.3 4.0 %copy-start.7 = (f32[1,128,2]{1,2,0:T(2,128)S(1)}, f32[1,128,2]{1,2,0:T(2,128)}, u32[]{:S(2)}) copy-start(f32[1,128,2]{1,2,0:T(2,128)} %param.29) | copy-start | bytes 3076
  240.3 51.6 %all-to-all-start.6 = ((bf16[8,64,2048]{2,1,0:T(8,128)(2,1)}), bf16[8,64,2048]{2,1,0:T(8,128)(2,1)S(1)}, u32[]{:S(2)}, u32[]{:S(2)}) async-start(bf16[8,64,2048]{2,1,0:T(8,128)(2,1)} %bitcast.130), calls=%async_computation.6 | async-start | bytes 4194304 | tf_op jit(solution)/shard_map/all_to_all | solution.py:159
  294.6 3.2 %copy-start.1 = (bf16[1,128,2048]{2,1,0:T(8,128)(2,1)S(1)}, bf16[1,128,2048]{2,1,0:T(8,128)(2,1)}, u32[]{:S(2)}) copy-start(bf16[1,128,2048]{2,1,0:T(8,128)(2,1)} %param.23) | copy-start | bytes 1572868
  294.6 3.2 %copy-start.2 = (f32[1,128,2048]{2,1,0:T(8,128)S(1)}, f32[1,128,2048]{2,1,0:T(8,128)}, u32[]{:S(2)}) copy-start(f32[1,128,2048]{2,1,0:T(8,128)} %copy.119) | copy-start | bytes 3145732
Sparse Core Ops, SparseCore 0:
  58.8 54.8 all-gather.4
  115.2 21.5 all-gather.2
where the time goes:
time: 306 us
  waiting for transfers between devices  123 us (40%)
  blocking collectives  81.4 us (27%)
  matrix products  35.4 us (12%)
  starting transfers between devices  22.2 us (7%)
  local copies, waits for them, and re-layouts  15.1 us (5%)
  other arithmetic  14.2 us (5%)
  between operations  13.8 us (5%)
    all_to_all x1, blocking collectives, on_device(): lax.all_to_all(buffer, 'sp', split_axis=0, concat_axis=0, tiled=True)  53.4 us
    all_to_all x1, waiting for transfers between devices, on_device(): lax.all_to_all(served, 'sp', split_axis=0, concat_axis=0, tiled=True)  46.2 us
    all_to_all x1, blocking collectives, on_device(): lax.all_to_all(by_heads, 'sp', split_axis=0, concat_axis=1, tiled=True)  28 us
    all_gather x1, waiting for transfers between devices, project_tokens(): all_rows = lax.all_gather(attended[None], 'dp', axis=0, tiled=True)  23.2 us
    dot_general x1, matrix products, on_device(): jnp.dot(hidden, expert_down[0], preferred_element_type=jnp.float32)  17 us
    all_to_all x1, waiting for transfers between devices, on_device(): lax.all_to_all(rot_query, 'sp', split_axis=1, concat_axis=0, tiled=True)  14.6 us
    all_to_all x1, waiting for transfers between devices, on_device(): lax.all_to_all(jnp.repeat(value_rows, group_size, axis=1), 'sp', split_ax...  13.7 us
    all_to_all x1, waiting for transfers between devices, on_device(): lax.all_to_all(jnp.repeat(rot_key, group_size, axis=1), 'sp', split_axis=...  11.4 us
  transfers between devices with their start and end apart: 7, of which 7 were waited for; matrix products, arithmetic and copies ran while one was open for 5% of the time, Pallas kernels for 0%

commit v1 on v0

--- a/solution.py
+++ b/solution.py
@@ -6,6 +6,30 @@
 GRID_W = 64
 EPS = 1e-06
 THETA = 10000.0
+
+
+def work_both_ways(x, axis, dim, work, out_dim):
+    size, mine, rows = (lax.axis_size(axis), lax.axis_index(axis), x.shape[dim])
+    right = [(i, (i + 1) % size) for i in range(size)]
+    left = [(b, a) for a, b in right]
+    lower, upper = (lax.ppermute(x, axis, right), lax.ppermute(x, axis, left))
+    made = work(x, mine * rows)
+    length = made.shape[out_dim]
+    out = jnp.zeros((*made.shape[:out_dim], size * length, *made.shape[out_dim + 1 :]), made.dtype)
+
+    def put(out, made, source):
+        return lax.dynamic_update_slice_in_dim(out, made, source * length, axis=out_dim)
+
+    out = put(out, made, mine)
+    for step in range(1, size // 2 + 1):
+        below, above = ((mine - step) % size, (mine + step) % size)
+        current = (lower, upper)
+        if step < size // 2:
+            lower, upper = (lax.ppermute(lower, axis, right), lax.ppermute(upper, axis, left))
+        out = put(out, work(current[0], below * rows), below)
+        if 2 * step < size:
+            out = put(out, work(current[1], above * rows), above)
+    return out
 
 
 def rotate_half(vector, position):
@@ -73,10 +97,15 @@
 
 
 def project_tokens(attended, out_weight):
-    all_rows = lax.all_gather(attended[None], "dp", axis=0, tiled=True)
     local_cols = lax.all_gather(out_weight, "sp", axis=0, tiled=True)
-    partial_cols = jnp.einsum(
-        "std,dc->stc", all_rows, local_cols, preferred_element_type=jnp.float32
+    partial_cols = work_both_ways(
+        attended[None],
+        "dp",
+        0,
+        lambda shard, start: jnp.einsum(
+            "std,dc->stc", shard, local_cols, preferred_element_type=jnp.float32
+        ),
+        0,
     )
     back_cols = lax.all_to_all(
         partial_cols.astype(jnp.bfloat16), "dp", split_axis=0, concat_axis=2, tiled=True

time: 306 us -> 293 us (0.958)
  blocking collectives: 81.4 us -> 52.9 us
  waiting for transfers between devices: 123 us -> 131 us
  starting transfers between devices: 22.2 us -> 28.2 us
    all_to_all x1 -> x0, blocking collectives: 28 us -> none  [on_device(): lax.all_to_all(by_heads, 'sp', split_axis=0, concat_axis=1, tiled=True)]
    all_to_all x0 -> x1, waiting for transfers between devices: none -> 24 us  [on_device(): lax.all_to_all(by_heads, 'sp', split_axis=0, concat_axis=1, tiled=True)]
    all_gather x1 -> x0, waiting for transfers between devices: 23.2 us -> none  [project_tokens(): all_rows = lax.all_gather(attended[None], 'dp', axis=0, tiled=True)]
    ppermute x0 -> x3, waiting for transfers between devices: none -> 11.4 us  [the longest x2 8.89 us: work_both_ways(): lower, upper = (lax.ppermute(x, axis, right), lax.ppermute(x, axis, left))]
    all_gather x1, waiting for transfers between devices: 5.06 us -> 0.01 us  [project_tokens(): local_cols = lax.all_gather(out_weight, 'sp', axis=0, tiled=True)]
    all_to_all x0 -> x1, starting transfers between devices: none -> 3.63 us  [on_device(): lax.all_to_all(by_heads, 'sp', split_axis=0, concat_axis=1, tiled=True)]
  transfers between devices with their start and end apart: 7 -> 10, of which waited for: 7 -> 8; matrix products, arithmetic and copies ran while one was open for 5% -> 7% of each run, Pallas kernels for 0% -> 0%
where the time goes in v1:
time: 293 us
  waiting for transfers between devices  131 us (45%)
  blocking collectives  52.9 us (18%)
  matrix products  37.2 us (13%)
  starting transfers between devices  28.2 us (10%)
  local copies, waits for them, and re-layouts  15.7 us (5%)
  other arithmetic  14.2 us (5%)
  between operations  13.9 us (5%)
    all_to_all x1, blocking collectives, on_device(): lax.all_to_all(buffer, 'sp', split_axis=0, concat_axis=0, tiled=True)  52.9 us
    all_to_all x1, waiting for transfers between devices, on_device(): lax.all_to_all(served, 'sp', split_axis=0, concat_axis=0, tiled=True)  46 us
    all_to_all x1, waiting for transfers between devices, on_device(): lax.all_to_all(by_heads, 'sp', split_axis=0, concat_axis=1, tiled=True)  24 us
    dot_general x1, matrix products, on_device(): jnp.dot(hidden, expert_down[0], preferred_element_type=jnp.float32)  17 us
    all_to_all x1, waiting for transfers between devices, on_device(): lax.all_to_all(rot_query, 'sp', split_axis=1, concat_axis=0, tiled=True)  14.6 us
    all_to_all x1, waiting for transfers between devices, on_device(): lax.all_to_all(jnp.repeat(value_rows, group_size, axis=1), 'sp', split_ax...  13.7 us
    all_to_all x1, waiting for transfers between devices, on_device(): lax.all_to_all(jnp.repeat(rot_key, group_size, axis=1), 'sp', split_axis=...  11.4 us
    dot_general x1, matrix products, on_device(): jnp.dot(flat_rows, expert_gate[0], preferred_element_type=jnp.float32)  9.45 us
  transfers between devices with their start and end apart: 10, of which 8 were waited for; matrix products, arithmetic and copies ran while one was open for 7% of the time, Pallas kernels for 0%

profile of v1, /device:TPU:0, one launch (start us, length us, event | category | flops | bytes accessed | tf_op | source)
XLA Modules:
  0.0 292.7 jit_solution(8233414892247400450)
XLA Ops:
  6.6 1.1 fusion.43
  7.7 1.1 fusion.44
  8.8 0.5 multiply_cosine_fusion.1
  9.4 0.5 subtract_convert_fusion.3
  9.9 0.4 pad_maximum_fusion.2
  10.3 0.9 broadcast_in_dim.17
  11.2 7.3 %all-to-all-start.1 = ((bf16[128,16,128]{2,0,1:T(8,128)(2,1)}), bf16[128,16,128]{2,0,1:T(8,128)(2,1)S(1)}, u32[]{:S(2)}, u32[]{:S(2)}) async-start(bf16[128,16,128]{2,0,1:T(8,128)(2,1)} %bitcast.12), calls=%async_computation.1 | async-start | bytes 1048576 | tf_op jit(solution)/shard_map/all_to_all | solution.py:141
  18.5 0.3 fusion.36
  18.9 0.3 fusion.37
  19.2 0.9 subtract_convert_fusion.1
  20.1 1.5 pad_maximum_fusion
  21.6 11.4 %all-to-all-done.1 = bf16[128,16,128]{2,0,1:T(8,128)(2,1)S(1)} async-done(((bf16[128,16,128]{2,0,1:T(8,128)(2,1)}), bf16[128,16,128]{2,0,1:T(8,128)(2,1)S(1)}, u32[]{:S(2)}, u32[]{:S(2)}) %all-to-all-start.1) | async-done | bytes 524320 | tf_op jit(solution)/shard_map/all_to_all | solution.py:141
  33.0 3.6 %all-to-all-start = ((bf16[128,16,128]{2,0,1:T(8,128)(2,1)}), bf16[128,16,128]{2,0,1:T(8,128)(2,1)S(1)}, u32[]{:S(2)}, u32[]{:S(2)}) async-start(bf16[128,16,128]{2,0,1:T(8,128)(2,1)} %pad_maximum_fusion), calls=%async_computation | async-start | bytes 1048576 | tf_op jit(solution)/shard_map/all_to_all | solution.py:140
  36.7 14.6 %all-to-all-done = bf16[128,16,128]{2,0,1:T(8,128)(2,1)S(1)} async-done(((bf16[128,16,128]{2,0,1:T(8,128)(2,1)}), bf16[128,16,128]{2,0,1:T(8,128)(2,1)S(1)}, u32[]{:S(2)}, u32[]{:S(2)}) %all-to-all-start) | async-done | bytes 524320 | tf_op jit(solution)/shard_map/all_to_all | solution.py:140
  51.3 0.9 broadcast_in_dim.18
  52.2 3.6 %all-to-all-start.2 = ((bf16[128,16,128]{2,0,1:T(8,128)(2,1)}), bf16[128,16,128]{2,0,1:T(8,128)(2,1)S(1)}, u32[]{:S(2)}, u32[]{:S(2)}) async-start(bf16[128,16,128]{2,0,1:T(8,128)(2,1)} %bitcast.18), calls=%async_computation.2 | async-start | bytes 1048576 | tf_op jit(solution)/shard_map/all_to_all | solution.py:144
  55.9 0.7 all-gather.2.cloned.1.call-update
  56.7 13.7 %all-to-all-done.2 = bf16[128,16,128]{2,0,1:T(8,128)(2,1)S(1)} async-done(((bf16[128,16,128]{2,0,1:T(8,128)(2,1)}), bf16[128,16,128]{2,0,1:T(8,128)(2,1)S(1)}, u32[]{:S(2)}, u32[]{:S(2)}) %all-to-all-start.2) | async-done | bytes 524320 | tf_op jit(solution)/shard_map/all_to_all | solution.py:144
  70.6 3.4 %while.20 = (s32[]{:T(128)}, bf16[2,512,128]{2,1,0:T(8,128)(2,1)S(1)}, bf16[2,512,128]{2,1,0:T(8,128)(2,1)S(1)}, bf16[1024,128]{1,0:T(8,128)(2,1)S(1)}, bf16[1024,128]{1,0:T(8,128)(2,1)S(1)}, /*index=5*/s32[]{:T(128)}) while((s32[]{:T(128)}, bf16[2,512,128]{2,1,0:T(8,128)(2,1)S(1)}, bf16[2,512,128]{2,1,0:T(8,128)(2,1)S(1)}, ...), condition=%wide.region_5.6_spmd, body=%wide.region_2.5_spmd.sunk | while | flops 273218560 | bytes 7088205 | solution.py:95
  70.6 0.5 multiply_reduce_fusion.6
  71.2 0.5 fusion.71
  71.7 0.7 fusion.72
  72.4 0.5 multiply_reduce_fusion.6
  72.9 0.5 fusion.71
  73.4 0.7 fusion.72
  74.1 3.5 %while.21 = (s32[]{:T(128)}, bf16[2,512,128]{2,1,0:T(8,128)(2,1)S(1)}, bf16[2,512,128]{2,1,0:T(8,128)(2,1)S(1)}, bf16[1024,128]{1,0:T(8,128)(2,1)S(1)}, bf16[1024,128]{1,0:T(8,128)(2,1)S(1)}, /*index=5*/s32[]{:T(128)}) while((s32[]{:T(128)}, bf16[2,512,128]{2,1,0:T(8,128)(2,1)S(1)}, bf16[2,512,128]{2,1,0:T(8,128)(2,1)S(1)}, ...), condition=%wide.region_9.10_spmd, body=%wide.region_6.9_spmd.sunk | while | flops 273218560 | bytes 7088205 | solution.py:95
  74.1 0.5 multiply_reduce_fusion.7
  74.7 0.5 fusion.75
  75.2 0.7 fusion.76
  75.9 0.5 multiply_reduce_fusion.7
  76.4 0.5 fusion.75
  76.9 0.7 fusion.76
  77.7 1.3 copy.111
  79.0 3.6 %all-to-all-start.3 = ((bf16[1024,2,128]{2,1,0:T(2,128)(2,1)}), bf16[1024,2,128]{2,1,0:T(2,128)(2,1)S(1)}, u32[]{:S(2)}, u32[]{:S(2)}) async-start(bf16[1024,2,128]{2,1,0:T(2,128)(2,1)} %copy.111), calls=%async_computation.3 | async-start | bytes 1048576 | tf_op jit(solution)/shard_map/all_to_all | solution.py:153
  82.9 24.0 %all-to-all-done.3 = bf16[1024,2,128]{2,1,0:T(2,128)(2,1)S(1)} async-done(((bf16[1024,2,128]{2,1,0:T(2,128)(2,1)}), bf16[1024,2,128]{2,1,0:T(2,128)(2,1)S(1)}, u32[]{:S(2)}, u32[]{:S(2)}) %all-to-all-start.3) | async-done | bytes 524320 | tf_op jit(solution)/shard_map/all_to_all | solution.py:153
  106.9 0.3 copy.113
  108.1 1.8 collective-permute-start.1
  109.9 8.9 %collective-permute-done = bf16[1,128,2048]{1,2,0:T(8,128)(2,1)S(1)} collective-permute-done((bf16[1,128,2048]{1,2,0:T(8,128)(2,1)S(1)}, bf16[1,128,2048]{1,2,0:T(8,128)(2,1)S(1)}, u32[]{:S(2)}, u32[]{:S(2)}) %collective-permute-start) | collective-permute-done | bytes 524320 | tf_op jit(solution)/shard_map/ppermute | solution.py:15
  118.8 0.3 collective-permute-start.2
  119.0 0.8 broadcast_in_dim.16
  119.9 2.7 fusion.30
  122.6 1.1 fusion.29
  123.7 1.1 fusion.28
  124.9 2.5 collective-permute-done.2
  127.4 1.1 fusion.27
  128.5 3.9 %all-to-all-start.4 = ((bf16[4,128,512]{2,1,0:T(8,128)(2,1)}), bf16[4,128,512]{2,1,0:T(8,128)(2,1)S(1)}, u32[]{:S(2)}, u32[]{:S(2)}) async-start(bf16[4,128,512]{2,1,0:T(8,128)(2,1)} %fusion.27), calls=%async_computation.4 | async-start | bytes 1048576 | tf_op jit(solution)/shard_map/all_to_all | solution.py:110
  132.5 8.7 %all-to-all-done.4 = bf16[4,128,512]{2,1,0:T(8,128)(2,1)S(1)} async-done(((bf16[4,128,512]{2,1,0:T(8,128)(2,1)}), bf16[4,128,512]{2,1,0:T(8,128)(2,1)S(1)}, u32[]{:S(2)}, u32[]{:S(2)}) %all-to-all-start.4) | async-done | bytes 524320 | tf_op jit(solution)/shard_map/all_to_all | solution.py:110
  141.4 0.3 copy.115
  141.7 0.3 copy.120
  142.0 0.4 copy-done.1
  142.4 0.2 multiply_reduce_fusion.3
  142.8 0.6 broadcast_in_dim.20
  143.5 1.2 reshape.326
  144.7 3.5 %scatter_custom_fusion = bf16[512,2048]{1,0:T(8,128)(2,1)S(1)} fusion(s32[256]{0:T(256)S(1)} %bitcast.169, bf16[256,2048]{1,0:T(8,128)(2,1)} %reshape.326, bf16[]{:T(256)} %constant.115.clone.1), kind=kCustom, calls=%fused_computation.55 | custom fusion | bytes 2097664 | tf_op jit(solution)/shard_map/scatter | solution.py:175
  148.2 52.9 %all_to_all.88 = bf16[8,64,2048]{2,1,0:T(8,128)(2,1)} all-to-all(bf16[8,64,2048]{2,1,0:T(8,128)(2,1)S(1)} %bitcast.152), channel_id=1, replica_groups=mesh['sp'=8,'dp'=4] {'sp'}, dimensions={0} | all-to-all | bytes 4194304 | tf_op jit(solution)/shard_map/all_to_all | solution.py:178
  201.1 9.5 %fusion.20 = f32[512,1792]{1,0:T(8,128)} fusion(bf16[512,2048]{1,0:T(8,128)(2,1)} %bitcast.49, bf16[1,2048,1792]{2,1,0:T(8,128)(2,1)} %param.25), kind=kOutput, calls=%fused_computation.30 | convolution fusion | flops 3758096384 | bytes 13107200 | tf_op jit(solution)/shard_map/dot_general | solution.py:181
  210.6 17.0 %fusion.24 = bf16[512,2048]{1,0:T(8,128)(2,1)} fusion(bf16[1,1792,2048]{2,1,0:T(8,128)(2,1)} %param.27, f32[512,1792]{1,0:T(8,128)} %fusion.20, bf16[512,2048]{1,0:T(8,128)(2,1)} %bitcast.49, bf16[1,2048,1792]{2,1,0:T(8,128)(2,1)} %param.26), kind=kOutput, calls=%fused_computation.33 | convolution fusion | flops 7522746368 | bytes 22544384 | tf_op jit(solution)/shard_map/dot_general | solution.py:184
  227.5 4.0 %all-to-all-start.6 = ((bf16[8,64,2048]{2,1,0:T(8,128)(2,1)}), bf16[8,64,2048]{2,1,0:T(8,128)(2,1)S(1)}, u32[]{:S(2)}, u32[]{:S(2)}) async-start(bf16[8,64,2048]{2,1,0:T(8,128)(2,1)} %bitcast.155), calls=%async_computation.6 | async-start | bytes 4194304 | tf_op jit(solution)/shard_map/all_to_all | solution.py:188
  231.6 1.3 copy.116
  232.9 46.0 %all-to-all-done.6 = bf16[8,64,2048]{2,1,0:T(8,128)(2,1)S(1)} async-done(((bf16[8,64,2048]{2,1,0:T(8,128)(2,1)}), bf16[8,64,2048]{2,1,0:T(8,128)(2,1)S(1)}, u32[]{:S(2)}, u32[]{:S(2)}) %all-to-all-start.6) | async-done | bytes 2097184 | tf_op jit(solution)/shard_map/all_to_all | solution.py:188
  278.9 1.4 gather_fusion
  280.3 1.3 reshape.311
  281.7 3.2 %multiply_reduce_fusion.2 = f32[128,2048]{1,0:T(8,128)S(1)} fusion(f32[128,2,2048]{2,1,0:T(2,128)S(1)} %reshape.311, f32[128,2]{1,0:T(8,128)S(1)} %copy.121), kind=kLoop, calls=%fused_computation.34 | loop fusion | flops 786432 | bytes 3146752 | tf_op jit(solution)/shard_map/reduce_sum | solution.py:194
  284.9 1.0 fusion.34
  (55 shorter events, 2.2 us)
Async XLA Ops:
  9.4 9.1 %copy-start.4 = (bf16[1,128,16,128]{3,2,1,0:T(8,128)(2,1)S(1)}, bf16[1,128,16,128]{3,2,1,0:T(8,128)(2,1)}, u32[]{:S(2)}) copy-start(bf16[1,128,16,128]{3,2,1,0:T(8,128)(2,1)} %param.17) | copy-start | bytes 1572868
  9.4 9.5 %copy-start.9 = (f32[128]{0:T(128)S(1)}, f32[128]{0:T(128)}, u32[]{:S(2)}) copy-start(f32[128]{0:T(128)} %param.20) | copy-start | bytes 1540
  11.2 21.8 %all-to-all-start.1 = ((bf16[128,16,128]{2,0,1:T(8,128)(2,1)}), bf16[128,16,128]{2,0,1:T(8,128)(2,1)S(1)}, u32[]{:S(2)}, u32[]{:S(2)}) async-start(bf16[128,16,128]{2,0,1:T(8,128)(2,1)} %bitcast.12), calls=%async_computation.1 | async-start | bytes 1048576 | tf_op jit(solution)/shard_map/all_to_all | solution.py:141
  20.1 16.5 %copy-start.5 = (bf16[1,128,4,128]{3,2,1,0:T(4,128)(2,1)S(1)}, bf16[1,128,4,128]{3,2,1,0:T(4,128)(2,1)}, u32[]{:S(2)}) copy-start(bf16[1,128,4,128]{3,2,1,0:T(4,128)(2,1)} %param.19) | copy-start | bytes 393220
  33.0 18.3 %all-to-all-start = ((bf16[128,16,128]{2,0,1:T(8,128)(2,1)}), bf16[128,16,128]{2,0,1:T(8,128)(2,1)S(1)}, u32[]{:S(2)}, u32[]{:S(2)}) async-start(bf16[128,16,128]{2,0,1:T(8,128)(2,1)} %pad_maximum_fusion), calls=%async_computation | async-start | bytes 1048576 | tf_op jit(solution)/shard_map/all_to_all | solution.py:140
  52.2 18.3 %all-to-all-start.2 = ((bf16[128,16,128]{2,0,1:T(8,128)(2,1)}), bf16[128,16,128]{2,0,1:T(8,128)(2,1)S(1)}, u32[]{:S(2)}, u32[]{:S(2)}) async-start(bf16[128,16,128]{2,0,1:T(8,128)(2,1)} %bitcast.18), calls=%async_computation.2 | async-start | bytes 1048576 | tf_op jit(solution)/shard_map/all_to_all | solution.py:144
  55.8 63.2 %all-gather.2.cloned.1.call-start = ((), (), s32[]{:S(2)}) async-start(), calls=%async_computation.7 | async-start | bytes 2359296 | tf_op jit(solution)/shard_map/all_gather | solution.py:100
  77.6 5.0 %copy-start.7 = (s32[1,128,2]{1,2,0:T(2,128)S(1)}, s32[1,128,2]{1,2,0:T(2,128)}, u32[]{:S(2)}) copy-start(s32[1,128,2]{1,2,0:T(2,128)} %param.28) | copy-start | bytes 3076
  79.0 27.9 %all-to-all-start.3 = ((bf16[1024,2,128]{2,1,0:T(2,128)(2,1)}), bf16[1024,2,128]{2,1,0:T(2,128)(2,1)S(1)}, u32[]{:S(2)}, u32[]{:S(2)}) async-start(bf16[1024,2,128]{2,1,0:T(2,128)(2,1)} %copy.111), calls=%async_computation.3 | async-start | bytes 1048576 | tf_op jit(solution)/shard_map/all_to_all | solution.py:153
  107.2 11.6 %collective-permute-start = (bf16[1,128,2048]{1,2,0:T(8,128)(2,1)S(1)}, bf16[1,128,2048]{1,2,0:T(8,128)(2,1)S(1)}, u32[]{:S(2)}, u32[]{:S(2)}) collective-permute-start(bf16[1,128,2048]{1,2,0:T(8,128)(2,1)S(1)} %bitcast.163), channel_id=1, source_target_pairs={{0,1},{1,2},{2,3},{3,0},{4,5},{5,6},{6,7},{7,4},{8,9},{9,10},{10,1... | collective-permute-start | bytes 1572872 | tf_op jit(solution)/shard_map/ppermute | solution.py:15
  108.1 15.6 %collective-permute-start.1 = (bf16[1,128,2048]{1,2,0:T(8,128)(2,1)S(1)}, bf16[1,128,2048]{1,2,0:T(8,128)(2,1)S(1)}, u32[]{:S(2)}, u32[]{:S(2)}) collective-permute-start(bf16[1,128,2048]{1,2,0:T(8,128)(2,1)S(1)} %bitcast.164), channel_id=1, source_target_pairs={{1,0},{2,1},{3,2},{0,3},{5,4},{6,5},{7,6},{4,7},{9,8},{10,9},{11,1... | collective-permute-start | bytes 1572872 | tf_op jit(solution)/shard_map/ppermute | solution.py:15
  118.8 8.6 %collective-permute-start.2 = (bf16[1,128,2048]{1,2,0:T(8,128)(2,1)S(1)}, bf16[1,128,2048]{1,2,0:T(8,128)(2,1)S(1)}, u32[]{:S(2)}, u32[]{:S(2)}) collective-permute-start(bf16[1,128,2048]{1,2,0:T(8,128)(2,1)S(1)} %collective-permute-done), channel_id=1, source_target_pairs={{0,1},{1,2},{2,3},{3,0},{4,5},{5,6},{6,7},{7,4},{8,9},{9,10},{10,1... | collective-permute-start | bytes 1572872 | tf_op jit(solution)/shard_map/ppermute | solution.py:28
  119.0 3.6 %copy-start = (bf16[2048,512]{1,0:T(8,128)(2,1)S(1)}, bf16[2048,512]{1,0:T(8,128)(2,1)}, u32[]{:S(2)}) copy-start(bf16[2048,512]{1,0:T(8,128)(2,1)} %all-gather.2.cloned.1.call-done) | copy-start | bytes 6291460
  128.5 12.7 %all-to-all-start.4 = ((bf16[4,128,512]{2,1,0:T(8,128)(2,1)}), bf16[4,128,512]{2,1,0:T(8,128)(2,1)S(1)}, u32[]{:S(2)}, u32[]{:S(2)}) async-start(bf16[4,128,512]{2,1,0:T(8,128)(2,1)} %fusion.27), calls=%async_computation.4 | async-start | bytes 1048576 | tf_op jit(solution)/shard_map/all_to_all | solution.py:110
  141.3 1.0 copy-start.1
  141.7 0.9 copy-start.6
  227.5 4.0 %copy-start.8 = (f32[1,128,2]{1,2,0:T(2,128)S(1)}, f32[1,128,2]{1,2,0:T(2,128)}, u32[]{:S(2)}) copy-start(f32[1,128,2]{1,2,0:T(2,128)} %param.29) | copy-start | bytes 3076
  227.5 51.4 %all-to-all-start.6 = ((bf16[8,64,2048]{2,1,0:T(8,128)(2,1)}), bf16[8,64,2048]{2,1,0:T(8,128)(2,1)S(1)}, u32[]{:S(2)}, u32[]{:S(2)}) async-start(bf16[8,64,2048]{2,1,0:T(8,128)(2,1)} %bitcast.155), calls=%async_computation.6 | async-start | bytes 4194304 | tf_op jit(solution)/shard_map/all_to_all | solution.py:188
  281.6 3.2 %copy-start.2 = (bf16[1,128,2048]{2,1,0:T(8,128)(2,1)S(1)}, bf16[1,128,2048]{2,1,0:T(8,128)(2,1)}, u32[]{:S(2)}) copy-start(bf16[1,128,2048]{2,1,0:T(8,128)(2,1)} %param.23) | copy-start | bytes 1572868
  281.7 3.2 %copy-start.3 = (f32[1,128,2048]{2,1,0:T(8,128)S(1)}, f32[1,128,2048]{2,1,0:T(8,128)}, u32[]{:S(2)}) copy-start(f32[1,128,2048]{2,1,0:T(8,128)} %copy.116) | copy-start | bytes 3145732
Sparse Core Ops, SparseCore 0:
  58.8 55.8 all-gather.1
